TPU v7x, 32 devices: a whole 2x2x4 slice. The times are simulated.
32 devices in a mesh: ep: 8 (over z, core), tp: 4 (over y, x).
Axes of the slice: x: 2, y: 2, z: 4, core: 2. Of those that a mesh axis runs over, the one named last changes fastest.
Arguments:
- tokens: bfloat16 [256, 4096], P('ep'), may hold values from -6 to 6
- recur_state: float32 [256, 4096], P('ep', 'tp'), may hold values from -6 to 6
- conv_state: bfloat16 [256, 3, 4096], P('ep', None, 'tp'), may hold values from -6 to 6
- mix_gain: float32 [4096], replicated, may hold values from 0.1 to 1.9
- in_weight: bfloat16 [4096, 4096], P('ep', 'tp'), may hold values from -0.09375 to 0.09375
- gate_weight: bfloat16 [4096, 4096], P('ep', 'tp'), may hold values from -0.09375 to 0.09375
- conv_taps: float32 [4, 4096], P(None, 'tp'), may hold values from -3 to 3
- recur_gate_blocks: bfloat16 [64, 64, 64], P('tp'), may hold values from -0.75 to 0.75
- input_gate_blocks: bfloat16 [64, 64, 64], P('tp'), may hold values from -0.75 to 0.75
- decay_rate: float32 [4096], P('tp'), may hold values from 0.01 to 0.4
- out_weight: bfloat16 [4096, 4096], P('tp', 'ep'), may hold values from -0.09375 to 0.09375
- ffn_gain: float32 [4096], replicated, may hold values from 0.1 to 1.9
- router_weight: bfloat16 [4096, 8], replicated, may hold values from -0.09375 to 0.09375
- routes: int32 [256, 2], P('ep'), may hold values from 0 to 7, as said below
- expert_gate: bfloat16 [8, 4096, 2048], P('ep', None, 'tp'), may hold values from -0.09375 to 0.09375
- expert_up: bfloat16 [8, 4096, 2048], P('ep', None, 'tp'), may hold values from -0.09375 to 0.09375
- expert_down: bfloat16 [8, 2048, 4096], P('ep', 'tp'), may hold values from -0.125 to 0.125
- dense_gate: bfloat16 [4096, 2048], P('ep', 'tp'), may hold values from -0.09375 to 0.09375
- dense_up: bfloat16 [4096, 2048], P('ep', 'tp'), may hold values from -0.09375 to 0.09375
- dense_down: bfloat16 [2048, 4096], P('tp', 'ep'), may hold values from -0.125 to 0.125
- branch_gate: bfloat16 [4096], replicated, may hold values from -0.09375 to 0.09375
Outputs:
- layer_out: bfloat16 [256, 4096], P('ep')
- new_state: float32 [256, 4096], P('ep', 'tp')
- new_conv_state: bfloat16 [256, 3, 4096], P('ep', None, 'tp')
Inputs may be any that keep to these rules, and one draw needn't show every extreme that they name: `routes`: A row names two different experts of one group: both have the same e // 4. In the rows of one index of ep no expert is named more than 16 times, and in every draw some expert is named exactly 16 times by the rows of every index of ep.
All inputs are finite; a program needn't handle non-finite values.
Results may differ from a plain program's by a relative error of at most 0.023.
Values may be sent and summed in bfloat16 or wider, within the bound.
A program may use at most 64 MiB of HBM per device.

v0:
```python
import jax
import jax.numpy as jnp
from jax import lax
from jax.sharding import PartitionSpec as P

TOP_K = 2
epsilon = 1e-06
decay_scale = 8.0


def rms_scale(rows, gain):
    values = rows.astype(jnp.float32)
    inverse = lax.rsqrt(jnp.mean(values * values, axis=-1, keepdims=True) + epsilon)
    return (values * inverse * gain).astype(jnp.bfloat16)


def on_device(
    tokens,
    recur_state,
    conv_state,
    mix_gain,
    in_weight,
    gate_weight,
    conv_taps,
    recur_gate_blocks,
    input_gate_blocks,
    decay_rate,
    out_weight,
    ffn_gain,
    router_weight,
    routes,
    expert_gate,
    expert_up,
    expert_down,
    dense_gate,
    dense_up,
    dense_down,
    branch_gate,
):
    batch_rows, width = tokens.shape
    channels = in_weight.shape[1]
    normed = rms_scale(tokens, mix_gain)
    arrived = lax.all_to_all(normed, "ep", split_axis=1, concat_axis=0, tiled=True)
    joined = jnp.concatenate([in_weight, gate_weight], axis=1)
    summed = lax.psum_scatter(
        jnp.dot(arrived, joined, preferred_element_type=jnp.float32).astype(jnp.bfloat16),
        "ep",
        scatter_dimension=0,
        tiled=True,
    ).astype(jnp.float32)
    x_sum, gate_sum = (summed[:, :channels], summed[:, channels:])
    x_branch = x_sum.astype(jnp.bfloat16)
    gate_branch = gate_sum.astype(jnp.bfloat16)
    window = jnp.concatenate([conv_state, x_branch[:, None, :]], axis=1)
    conv_out = jnp.sum(window.astype(jnp.float32) * conv_taps[None], axis=1).astype(jnp.bfloat16)
    new_conv_state = window[:, 1:, :]
    blocks = conv_out.reshape(batch_rows, recur_gate_blocks.shape[0], recur_gate_blocks.shape[1])
    recur_gate = jax.nn.sigmoid(
        jnp.einsum(
            "bhi,hij->bhj", blocks, recur_gate_blocks, preferred_element_type=jnp.float32
        ).reshape(batch_rows, channels)
    )
    input_gate = jax.nn.sigmoid(
        jnp.einsum(
            "bhi,hij->bhj", blocks, input_gate_blocks, preferred_element_type=jnp.float32
        ).reshape(batch_rows, channels)
    )
    log_decay = -decay_scale * recur_gate * decay_rate
    new_state = jnp.exp(log_decay) * recur_state + jnp.sqrt(
        -jnp.expm1(2.0 * log_decay)
    ) * input_gate * conv_out.astype(jnp.float32)
    mixer_rows = (new_state * jax.nn.gelu(gate_branch.astype(jnp.float32))).astype(jnp.bfloat16)
    mixer_part = jnp.dot(
        mixer_rows,
        lax.all_gather(out_weight, "ep", axis=1, tiled=True),
        preferred_element_type=jnp.float32,
    )
    resid = (
        tokens.astype(jnp.float32)
        + lax.psum(mixer_part.astype(jnp.bfloat16), "tp").astype(jnp.float32)
    ).astype(jnp.bfloat16)
    normed_ffn = rms_scale(resid, ffn_gain)
    router_logits = jnp.dot(normed_ffn, router_weight, preferred_element_type=jnp.float32)
    experts = router_logits.shape[1]
    expert_ids = lax.broadcasted_iota(jnp.int32, (batch_rows, TOP_K, experts), 2)
    picked = jnp.sum(
        jnp.where(routes[:, :, None] == expert_ids, router_logits[:, None, :], 0.0), axis=2
    )
    route_weight = jax.nn.sigmoid(picked - picked[:, ::-1]).astype(jnp.bfloat16)
    capacity = 2 * batch_rows * TOP_K // experts
    flat_ids = routes.reshape(batch_rows * TOP_K)
    onehot = (
        flat_ids[:, None] == lax.broadcasted_iota(jnp.int32, (batch_rows * TOP_K, experts), 1)
    ).astype(jnp.int32)
    rank = jnp.sum((jnp.cumsum(onehot, axis=0) - onehot) * onehot, axis=1)
    slot_of = (flat_ids * capacity + rank).reshape(batch_rows, TOP_K)
    slot_rows = lax.broadcasted_iota(jnp.int32, (experts * capacity, batch_rows), 0)
    slot_cols = lax.broadcasted_iota(jnp.int32, (batch_rows, experts * capacity), 1)
    dispatch = jnp.zeros((experts * capacity, batch_rows), jnp.bfloat16)
    combine = jnp.zeros((batch_rows, experts * capacity), jnp.bfloat16)
    for pick in range(TOP_K):
        dispatch = dispatch + (slot_rows == slot_of[None, :, pick]).astype(jnp.bfloat16)
        combine = combine + jnp.where(
            slot_cols == slot_of[:, pick : pick + 1],
            route_weight[:, pick : pick + 1],
            jnp.zeros((), jnp.bfloat16),
        )
    outgoing = (
        jnp.dot(dispatch, normed_ffn, preferred_element_type=jnp.float32)
        .astype(jnp.bfloat16)
        .reshape(experts, capacity, width)
    )
    gate_local = expert_gate[0]
    up_local = expert_up[0]
    down_local = expert_down[0]
    arrived_rows = lax.all_to_all(outgoing, "ep", split_axis=0, concat_axis=0, tiled=True)
    sources, items, features = arrived_rows.shape
    rows = arrived_rows.reshape(sources * items, features)
    first = jnp.dot(rows, gate_local, preferred_element_type=jnp.float32)
    second = jnp.dot(rows, up_local, preferred_element_type=jnp.float32)
    act = (jax.nn.silu(first) * second).astype(jnp.bfloat16)
    partial_value = jnp.dot(act, down_local, preferred_element_type=jnp.float32)
    total = lax.psum(partial_value.astype(jnp.bfloat16), "tp")
    returned = lax.all_to_all(
        total.reshape(sources, items, total.shape[1]), "ep", split_axis=0, concat_axis=0, tiled=True
    )
    moe = jnp.dot(
        combine,
        returned.reshape(experts * capacity, returned.shape[2]),
        preferred_element_type=jnp.float32,
    )
    dense_arrived = lax.all_to_all(normed_ffn, "ep", split_axis=1, concat_axis=0, tiled=True)
    dense_joined = jnp.concatenate([dense_gate, dense_up], axis=1)
    dense_summed = lax.psum_scatter(
        jnp.dot(dense_arrived, dense_joined, preferred_element_type=jnp.float32).astype(
            jnp.bfloat16
        ),
        "ep",
        scatter_dimension=0,
        tiled=True,
    ).astype(jnp.float32)
    dense_first = dense_summed[:, : dense_gate.shape[1]]
    dense_second = dense_summed[:, dense_gate.shape[1] :]
    dense_act = (jax.nn.silu(dense_first) * dense_second).astype(jnp.bfloat16)
    dense_part = jnp.dot(
        dense_act,
        lax.all_gather(dense_down, "ep", axis=1, tiled=True),
        preferred_element_type=jnp.float32,
    )
    branch_weight = jax.nn.sigmoid(
        jnp.dot(normed_ffn, branch_gate, preferred_element_type=jnp.float32)
    )
    dense_sum = lax.psum(dense_part.astype(jnp.bfloat16), "tp").astype(jnp.float32)
    layer_out = (resid.astype(jnp.float32) + moe + branch_weight[:, None] * dense_sum).astype(
        jnp.bfloat16
    )
    return (layer_out, new_state, new_conv_state)


def solution(mesh):
    in_specs = (
        P("ep", None),
        P("ep", "tp"),
        P("ep", None, "tp"),
        P(),
        P("ep", "tp"),
        P("ep", "tp"),
        P(None, "tp"),
        P("tp", None, None),
        P("tp", None, None),
        P("tp"),
        P("tp", "ep"),
        P(),
        P(),
        P("ep", None),
        P("ep", None, "tp"),
        P("ep", None, "tp"),
        P("ep", "tp", None),
        P("ep", "tp"),
        P("ep", "tp"),
        P("tp", "ep"),
        P(),
    )
    out_specs = (P("ep", None), P("ep", "tp"), P("ep", None, "tp"))
    return jax.shard_map(
        on_device, mesh=mesh, in_specs=in_specs, out_specs=out_specs, check_vma=False
    )
```

profile of v0, /device:TPU:0, one launch (start us, length us, event | category | flops | bytes accessed | tf_op | source)
XLA Modules:
  0.0 396.9 jit_solution(11186199223250125864)
XLA Ops:
  7.2 1.1 fusion.33
  8.4 1.1 fusion.35
  9.5 16.0 %all_to_all.48 = bf16[32,8,512]{2,0,1:T(8,128)(2,1)S(1)} all-to-all(bf16[32,8,512]{2,0,1:T(8,128)(2,1)S(1)} %bitcast.77), channel_id=1, replica_groups=mesh['ep'=8,'tp'=4] {'ep'}, dimensions={1} | all-to-all | bytes 524288 | tf_op jit(solution)/shard_map/all_to_all | solution.py:43
  25.5 3.4 convolution_convert_fusion.4
  29.0 0.7 all-gather.3.cloned.1.call-update
  29.8 30.9 %reduce-scatter.3.cloned.1.call-done = bf16[32,2048]{1,0:T(8,128)(2,1)} async-done(((bf16[256,2048]{1,0:T(8,128)(2,1)}), bf16[32,2048]{1,0:T(8,128)(2,1)}) %reduce-scatter.3.cloned.1.call-update) | async-done | bytes 131088 | tf_op jit(solution)/shard_map/reduce_scatter | solution.py:45
  60.7 0.9 slice_bitcast_fusion
  61.9 0.2 fusion.17
  62.4 0.2 fusion.13
  63.1 79.5 %all-gather.3.cloned.1.call-done = bf16[1024,4096]{1,0:T(8,128)(2,1)} async-done(((bf16[1024,512]{1,0:T(8,128)(2,1)}), bf16[1024,4096]{1,0:T(8,128)(2,1)}) %all-gather.3.cloned.1.call-update) | async-done | bytes 8388624 | tf_op jit(solution)/shard_map/all_gather | solution.py:75
  142.5 5.6 %convolution_convert_fusion.3 = bf16[32,4096]{1,0:T(8,128)(2,1)} fusion(bf16[1024,4096]{1,0:T(8,128)(2,1)} %all-gather.3.cloned.1.call-done, f32[32,1024]{1,0:T(8,128)S(1)} %multiply_add_fusion, bf16[32,2048]{1,0:T(8,128)(2,1)S(1)} %copy-done.5), kind=kOutput, calls=%fused_computation.6 | convolution fusion | flops 268926976 | bytes 8847360 | tf_op jit(solution)/shard_map/dot_general | solution.py:73
  148.2 41.6 %all-reduce.4.cloned.1.call-done = bf16[32,4096]{1,0:T(8,128)(2,1)} async-done(((bf16[32,4096]{1,0:T(8,128)(2,1)}), bf16[32,4096]{1,0:T(8,128)(2,1)}) %all-reduce.4.cloned.1.call-update) | async-done | bytes 262160 | tf_op jit(solution)/shard_map/psum | solution.py:80
  189.9 1.1 fusion.37
  191.0 1.1 fusion.39
  192.1 14.1 %all_to_all.49 = bf16[32,8,512]{2,0,1:T(8,128)(2,1)S(1)} all-to-all(bf16[32,8,512]{2,0,1:T(8,128)(2,1)S(1)} %bitcast.78), channel_id=1, replica_groups=mesh['ep'=8,'tp'=4] {'ep'}, dimensions={1} | all-to-all | bytes 524288 | tf_op jit(solution)/shard_map/all_to_all | solution.py:132
  206.2 1.3 convolution_convert_fusion.5
  207.6 0.5 all-gather.5.cloned.1.call-update
  208.5 0.2 select_reduce_fusion
  208.9 1.4 convolution_convert_fusion.1
  210.3 3.6 all-to-all-start.1
  213.9 24.5 %reduce-scatter.5.cloned.1.call-done = bf16[32,1024]{1,0:T(8,128)(2,1)} async-done(((bf16[256,1024]{1,0:T(8,128)(2,1)}), bf16[32,1024]{1,0:T(8,128)(2,1)}) %reduce-scatter.5.cloned.1.call-update) | async-done | bytes 65552 | tf_op jit(solution)/shard_map/reduce_scatter | solution.py:134
  238.4 0.8 convert_element_type.109
  239.2 49.8 %all-gather.5.cloned.1.call-done = bf16[512,4096]{1,0:T(8,128)(2,1)} async-done(((bf16[512,512]{1,0:T(8,128)(2,1)}), bf16[512,4096]{1,0:T(8,128)(2,1)}) %all-gather.5.cloned.1.call-update) | async-done | bytes 4194320 | tf_op jit(solution)/shard_map/all_gather | solution.py:147
  289.0 3.7 convolution_convert_fusion.2
  292.7 2.9 fusion.5
  295.7 5.9 %convolution_convert_fusion = bf16[128,4096]{1,0:T(8,128)(2,1)} fusion(bf16[1,512,4096]{2,1,0:T(8,128)(2,1)} %param.37, bf16[128,4096]{1,0:T(8,128)(2,1)S(1)} %bitcast.72, bf16[1,4096,512]{2,1,0:T(8,128)(2,1)} %param.36, f32[128,512]{1,0:T(8,128)S(1)} %fusion.5), kind=kOutput, calls=%fused_computation | convolution fusion | flops 1074659328 | bytes 10747904 | tf_op jit(solution)/shard_map/dot_general | solution.py:122
  301.6 55.4 %all-reduce.6.cloned.1.call-done = (bf16[8,16,4096]{2,1,0:T(8,128)(2,1)}, bf16[32,4096]{1,0:T(8,128)(2,1)}) async-done(((bf16[8,16,4096]{2,1,0:T(8,128)(2,1)}, bf16[32,4096]{1,0:T(8,128)(2,1)}), (bf16[8,16,4096]{2,1,0:T(8,128)(2,1)}, bf16[32,4096]{1,0:T(8,128)(2,1)})) %all-reduce.6.cloned.1.call-update) | async-done | bytes 1310736 | tf_op jit(solution)/shard_map/psum | solution.py:123
  356.9 4.6 %all-to-all-start.2 = ((bf16[8,16,4096]{2,1,0:T(8,128)(2,1)}), bf16[8,16,4096]{2,1,0:T(8,128)(2,1)S(1)}, u32[]{:S(2)}, u32[]{:S(2)}) async-start(bf16[8,16,4096]{2,1,0:T(8,128)(2,1)} %get-tuple-element.3), calls=%async_computation.3 | async-start | bytes 2097152 | tf_op jit(solution)/shard_map/all_to_all | solution.py:124
  361.5 0.7 fusion.45
  362.5 0.2 fusion.27
  362.7 25.4 %all-to-all-done.2 = bf16[8,16,4096]{2,1,0:T(8,128)(2,1)S(1)} async-done(((bf16[8,16,4096]{2,1,0:T(8,128)(2,1)}), bf16[8,16,4096]{2,1,0:T(8,128)(2,1)S(1)}, u32[]{:S(2)}, u32[]{:S(2)}) %all-to-all-start.2) | async-done | bytes 1048608 | tf_op jit(solution)/shard_map/all_to_all | solution.py:124
  388.1 2.0 fusion.1
  (69 shorter events, 2.2 us)
Async XLA Ops:
  7.2 54.7 %copy-start = (bf16[16,64,64]{2,1,0:T(8,128)(2,1)S(1)}, bf16[16,64,64]{2,1,0:T(8,128)(2,1)}, u32[]{:S(2)}) copy-start(bf16[16,64,64]{2,1,0:T(8,128)(2,1)} %param.28) | copy-start | bytes 393220
  7.2 53.5 %reduce-scatter.3.cloned.1.call-start = ((), (), s32[]{:S(2)}) async-start(), calls=%async_computation.6 | async-start | bytes 1179648 | tf_op jit(solution)/shard_map/reduce_scatter | solution.py:45
  8.4 21.4 %copy-start.12 = (f32[1024]{0:T(1024)S(1)}, f32[1024]{0:T(1024)}, u32[]{:S(2)}) copy-start(f32[1024]{0:T(1024)} %param.30) | copy-start | bytes 12292
  9.5 52.1 %copy-start.4 = (bf16[32,3,1024]{2,0,1:T(8,128)(2,1)S(1)}, bf16[32,3,1024]{2,0,1:T(8,128)(2,1)}, u32[]{:S(2)}) copy-start(bf16[32,3,1024]{2,0,1:T(8,128)(2,1)} %param.23) | copy-start | bytes 589828
  9.5 52.1 %copy-start.9 = (f32[4,1024]{1,0:T(4,128)S(1)}, f32[4,1024]{1,0:T(4,128)}, u32[]{:S(2)}) copy-start(f32[4,1024]{1,0:T(4,128)} %param.27) | copy-start | bytes 49156
  25.5 36.8 %copy-start.15 = (bf16[16,64,64]{2,1,0:T(8,128)(2,1)S(1)}, bf16[16,64,64]{2,1,0:T(8,128)(2,1)}, u32[]{:S(2)}) copy-start(bf16[16,64,64]{2,1,0:T(8,128)(2,1)} %param.29) | copy-start | bytes 393220
  28.9 34.0 %copy-start.6 = (f32[32,1024]{1,0:T(8,128)S(1)}, f32[32,1024]{1,0:T(8,128)}, u32[]{:S(2)}) copy-start(f32[32,1024]{1,0:T(8,128)} %param.22) | copy-start | bytes 393220
  28.9 113.6 %all-gather.3.cloned.1.call-start = ((), (), s32[]{:S(2)}) async-start(), calls=%async_computation.7 | async-start | bytes 9437184 | tf_op jit(solution)/shard_map/all_gather | solution.py:75
  29.7 160.2 %all-reduce.4.cloned.1.call-start = ((), (), s32[]{:S(2)}) async-start(), calls=%async_computation.8 | async-start | bytes 524288 | tf_op jit(solution)/shard_map/psum | solution.py:80
  60.7 81.8 %copy-start.5 = (bf16[32,2048]{1,0:T(8,128)(2,1)S(1)}, bf16[32,2048]{1,0:T(8,128)(2,1)}, u32[]{:S(2)}) copy-start(bf16[32,2048]{1,0:T(8,128)(2,1)} %reduce-scatter.3.cloned.1.call-done) | copy-start | bytes 393220
  63.0 85.1 %copy-start.3 = (f32[32,1024]{1,0:T(8,128)}, f32[32,1024]{1,0:T(8,128)S(1)}, u32[]{:S(2)}) copy-start(f32[32,1024]{1,0:T(8,128)S(1)} %multiply_add_fusion) | copy-start | bytes 393220
  63.0 126.8 %copy-start.1 = (bf16[32,4096]{1,0:T(8,128)(2,1)S(1)}, bf16[32,4096]{1,0:T(8,128)(2,1)}, u32[]{:S(2)}) copy-start(bf16[32,4096]{1,0:T(8,128)(2,1)} %param.21) | copy-start | bytes 786436
  63.0 128.0 %copy-start.8 = (f32[4096]{0:T(1024)S(1)}, f32[4096]{0:T(1024)}, u32[]{:S(2)}) copy-start(f32[4096]{0:T(1024)} %param.32) | copy-start | bytes 49156
  63.1 143.2 %copy-start.13 = (bf16[512,512]{1,0:T(8,128)(2,1)S(1)}, bf16[512,512]{1,0:T(8,128)(2,1)}, u32[]{:S(2)}) copy-start(bf16[512,512]{1,0:T(8,128)(2,1)} %param.39) | copy-start | bytes 1572868
  63.1 143.2 %copy-start.14 = (bf16[512,512]{1,0:T(8,128)(2,1)S(1)}, bf16[512,512]{1,0:T(8,128)(2,1)}, u32[]{:S(2)}) copy-start(bf16[512,512]{1,0:T(8,128)(2,1)} %param.38) | copy-start | bytes 1572868
  148.2 60.0 %copy-start.10 = (s32[32,2]{0,1:T(2,128)S(1)}, s32[32,2]{0,1:T(2,128)}, u32[]{:S(2)}) copy-start(s32[32,2]{0,1:T(2,128)} %param.34) | copy-start | bytes 772
  148.2 90.2 %reduce-scatter.5.cloned.1.call-start = ((), (), s32[]{:S(2)}) async-start(), calls=%async_computation.9 | async-start | bytes 589824 | tf_op jit(solution)/shard_map/reduce_scatter | solution.py:134
  207.6 81.4 %all-gather.5.cloned.1.call-start = ((), (), s32[]{:S(2)}) async-start(), calls=%async_computation.10 | async-start | bytes 4718592 | tf_op jit(solution)/shard_map/all_gather | solution.py:147
  210.3 82.4 %all-to-all-start.1 = ((bf16[8,16,4096]{2,1,0:T(8,128)(2,1)}), bf16[8,16,4096]{2,1,0:T(8,128)(2,1)S(1)}, u32[]{:S(2)}, u32[]{:S(2)}) async-start(bf16[8,16,4096]{2,1,0:T(8,128)(2,1)} %bitcast.9), calls=%async_computation.2 | async-start | bytes 2097152 | tf_op jit(solution)/shard_map/all_to_all | solution.py:116
  213.9 143.0 %all-reduce.6.cloned.1.call-start = ((), (), s32[]{:S(2)}) async-start(), calls=%async_computation.11 | async-start | bytes 2621440 | tf_op jit(solution)/shard_map/psum | solution.py:123
  295.6 65.9 %copy-start.11 = (bf16[4096]{0:T(1024)(128)(2,1)S(1)}, bf16[4096]{0:T(1024)(128)(2,1)}, u32[]{:S(2)}) copy-start(bf16[4096]{0:T(1024)(128)(2,1)} %param.41) | copy-start | bytes 24580
  295.6 66.6 %copy-start.7 = (bf16[4096,8]{0,1:T(8,128)(2,1)S(1)}, bf16[4096,8]{0,1:T(8,128)(2,1)}, u32[]{:S(2)}) copy-start(bf16[4096,8]{0,1:T(8,128)(2,1)} %param.33) | copy-start | bytes 196612
  301.5 86.5 %copy-start.2 = (bf16[32,4096]{1,0:T(8,128)(2,1)S(1)}, bf16[32,4096]{1,0:T(8,128)(2,1)}, u32[]{:S(2)}) copy-start(bf16[32,4096]{1,0:T(8,128)(2,1)} %all-reduce.4.cloned.1.call-done) | copy-start | bytes 786436
  356.9 31.2 %all-to-all-start.2 = ((bf16[8,16,4096]{2,1,0:T(8,128)(2,1)}), bf16[8,16,4096]{2,1,0:T(8,128)(2,1)S(1)}, u32[]{:S(2)}, u32[]{:S(2)}) async-start(bf16[8,16,4096]{2,1,0:T(8,128)(2,1)} %get-tuple-element.3), calls=%async_computation.3 | async-start | bytes 2097152 | tf_op jit(solution)/shard_map/all_to_all | solution.py:124
Sparse Core Ops, SparseCore 0:
  29.1 31.6 reduce-scatter.2
  62.3 80.1 all-gather.2
  148.3 41.5 all-reduce.3
  207.7 30.6 reduce-scatter.4
  239.8 49.1 all-gather.4
  301.7 55.1 all-reduce.5
where the time goes:
time: 398 us; the launch traced here: 397 us
  waiting for transfers between devices  308 us (77%)
  blocking collectives  30.1 us (8%)
  matrix products  26.9 us (7%)
  between operations  14.4 us (4%)
  starting transfers between devices  8.4 us (2%)
  other arithmetic  6.59 us (2%)
    all_gather x1, waiting for transfers between devices, on_device(): lax.all_gather(out_weight, 'ep', axis=1, tiled=True)  79.5 us
    psum x1, waiting for transfers between devices, on_device(): total = lax.psum(partial_value.astype(jnp.bfloat16), 'tp')  55.4 us
    all_gather x1, waiting for transfers between devices, on_device(): lax.all_gather(dense_down, 'ep', axis=1, tiled=True)  49.8 us
    psum x1, waiting for transfers between devices, on_device(): lax.psum(mixer_part.astype(jnp.bfloat16), 'tp').astype(jnp.float32)  41.6 us
    reduce_scatter x1, waiting for transfers between devices, on_device(): lax.psum_scatter(jnp.dot(arrived, joined, preferred_element_type=jnp.floa...  30.9 us
    all_to_all x1, waiting for transfers between devices, on_device(): lax.all_to_all(total.reshape(sources, items, total.shape[1]), 'ep', split...  25.4 us
    reduce_scatter x1, waiting for transfers between devices, on_device(): lax.psum_scatter(jnp.dot(dense_arrived, dense_joined, preferred_element_t...  24.5 us
    all_to_all x1, blocking collectives, on_device(): lax.all_to_all(normed, 'ep', split_axis=1, concat_axis=0, tiled=True)  16 us
  transfers between devices with their start and end apart: 8, of which 7 were waited for; matrix products, arithmetic and copies ran while one was open for 3% of the time, Pallas kernels for 0%

commit v1 on v0

--- a/solution.py
+++ b/solution.py
@@ -1,3 +1,4 @@
+import functools
 import jax
 import jax.numpy as jnp
 from jax import lax
@@ -6,6 +7,14 @@
 TOP_K = 2
 epsilon = 1e-06
 decay_scale = 8.0
+
+
+def launch_weights(view, axis_name):
+    current_arr = jnp.sum(lax.all_gather(view, axis_name), axis=0)
+    return current_arr
+
+
+rings_time = functools.partial(launch_weights, axis_name="tp")
 
 
 def rms_scale(rows, gain):
@@ -76,8 +85,7 @@
         preferred_element_type=jnp.float32,
     )
     resid = (
-        tokens.astype(jnp.float32)
-        + lax.psum(mixer_part.astype(jnp.bfloat16), "tp").astype(jnp.float32)
+        tokens.astype(jnp.float32) + rings_time(mixer_part.astype(jnp.bfloat16)).astype(jnp.float32)
     ).astype(jnp.bfloat16)
     normed_ffn = rms_scale(resid, ffn_gain)
     router_logits = jnp.dot(normed_ffn, router_weight, preferred_element_type=jnp.float32)

time: 398 us -> 380 us (0.955)
  waiting for transfers between devices: 308 us -> 292 us
    psum x1 -> x0, waiting for transfers between devices: 41.6 us -> none  [on_device(): lax.psum(mixer_part.astype(jnp.bfloat16), 'tp').astype(jnp.float32)]
    all_gather x0 -> x1, waiting for transfers between devices: none -> 25.1 us  [launch_weights(): current_arr = jnp.sum(lax.all_gather(view, axis_name), axis=0)]
where the time goes in v1:
time: 380 us
  waiting for transfers between devices  292 us (77%)
  blocking collectives  30.1 us (8%)
  matrix products  26.9 us (7%)
  between operations  14.4 us (4%)
  starting transfers between devices  8.4 us (2%)
  other arithmetic  6.12 us (2%)
    all_gather x1, waiting for transfers between devices, on_device(): lax.all_gather(out_weight, 'ep', axis=1, tiled=True)  79.4 us
    psum x1, waiting for transfers between devices, on_device(): total = lax.psum(partial_value.astype(jnp.bfloat16), 'tp')  55.4 us
    all_gather x1, waiting for transfers between devices, on_device(): lax.all_gather(dense_down, 'ep', axis=1, tiled=True)  49.7 us
    reduce_scatter x1, waiting for transfers between devices, on_device(): lax.psum_scatter(jnp.dot(arrived, joined, preferred_element_type=jnp.floa...  30.9 us
    all_to_all x1, waiting for transfers between devices, on_device(): lax.all_to_all(total.reshape(sources, items, total.shape[1]), 'ep', split...  25.4 us
    all_gather x1, waiting for transfers between devices, launch_weights(): current_arr = jnp.sum(lax.all_gather(view, axis_name), axis=0)  25.1 us
    reduce_scatter x1, waiting for transfers between devices, on_device(): lax.psum_scatter(jnp.dot(dense_arrived, dense_joined, preferred_element_t...  24.5 us
    all_to_all x1, blocking collectives, on_device(): lax.all_to_all(normed, 'ep', split_axis=1, concat_axis=0, tiled=True)  16 us
  transfers between devices with their start and end apart: 8, of which 7 were waited for; matrix products, arithmetic and copies ran while one was open for 3% of the time, Pallas kernels for 0%

profile of v1, /device:TPU:0, one launch (start us, length us, event | category | flops | bytes accessed | tf_op | source)
XLA Modules:
  0.0 379.8 jit_solution(14939767746100767703)
XLA Ops:
  7.2 1.1 fusion.33
  8.4 1.1 fusion.35
  9.5 16.0 %all_to_all.48 = bf16[32,8,512]{2,0,1:T(8,128)(2,1)S(1)} all-to-all(bf16[32,8,512]{2,0,1:T(8,128)(2,1)S(1)} %bitcast.79), channel_id=1, replica_groups=mesh['ep'=8,'tp'=4] {'ep'}, dimensions={1} | all-to-all | bytes 524288 | tf_op jit(solution)/shard_map/all_to_all | solution.py:52
  25.5 3.4 convolution_convert_fusion.4
  29.0 0.7 all-gather.5.cloned.1.call-update
  29.7 30.9 %reduce-scatter.3.cloned.1.call-done = bf16[32,2048]{1,0:T(8,128)(2,1)} async-done(((bf16[256,2048]{1,0:T(8,128)(2,1)}), bf16[32,2048]{1,0:T(8,128)(2,1)}) %reduce-scatter.3.cloned.1.call-update) | async-done | bytes 131088 | tf_op jit(solution)/shard_map/reduce_scatter | solution.py:54
  60.7 0.9 slice_bitcast_fusion
  61.8 0.2 fusion.17
  62.4 0.2 fusion.13
  63.1 79.4 %all-gather.5.cloned.1.call-done = bf16[1024,4096]{1,0:T(8,128)(2,1)} async-done(((bf16[1024,512]{1,0:T(8,128)(2,1)}), bf16[1024,4096]{1,0:T(8,128)(2,1)}) %all-gather.5.cloned.1.call-update) | async-done | bytes 8388624 | tf_op jit(solution)/shard_map/all_gather | solution.py:84
  142.5 5.6 %convolution_convert_fusion.3 = bf16[32,4096]{1,0:T(8,128)(2,1)} fusion(bf16[1024,4096]{1,0:T(8,128)(2,1)} %all-gather.5.cloned.1.call-done, f32[32,1024]{1,0:T(8,128)S(1)} %multiply_add_fusion, bf16[32,2048]{1,0:T(8,128)(2,1)S(1)} %copy-done.4), kind=kOutput, calls=%fused_computation.6 | convolution fusion | flops 268926976 | bytes 8847360 | tf_op jit(solution)/shard_map/dot_general | solution.py:82
  148.2 25.1 %all-gather.9.cloned.1.call-done = bf16[128,4096]{1,0:T(8,128)(2,1)} async-done(((bf16[32,4096]{1,0:T(8,128)(2,1)}), bf16[128,4096]{1,0:T(8,128)(2,1)}) %all-gather.9.cloned.1.call-update) | async-done | bytes 1048592 | tf_op jit(solution)/shard_map/all_gather | solution.py:13
  173.3 1.4 reduce_sum.61
  174.7 0.2 fusion.37
  175.1 14.1 %all_to_all.49 = bf16[32,8,512]{2,0,1:T(8,128)(2,1)S(1)} all-to-all(bf16[32,8,512]{2,0,1:T(8,128)(2,1)S(1)} %bitcast.80), channel_id=1, replica_groups=mesh['ep'=8,'tp'=4] {'ep'}, dimensions={1} | all-to-all | bytes 524288 | tf_op jit(solution)/shard_map/all_to_all | solution.py:140
  189.2 1.3 convolution_convert_fusion.5
  190.6 0.5 all-gather.7.cloned.1.call-update
  191.5 0.2 select_reduce_fusion
  191.9 1.4 convolution_convert_fusion.1
  193.3 3.6 all-to-all-start.1
  196.9 24.5 %reduce-scatter.5.cloned.1.call-done = bf16[32,1024]{1,0:T(8,128)(2,1)} async-done(((bf16[256,1024]{1,0:T(8,128)(2,1)}), bf16[32,1024]{1,0:T(8,128)(2,1)}) %reduce-scatter.5.cloned.1.call-update) | async-done | bytes 65552 | tf_op jit(solution)/shard_map/reduce_scatter | solution.py:142
  221.3 0.8 convert_element_type.111
  222.2 49.7 %all-gather.7.cloned.1.call-done = bf16[512,4096]{1,0:T(8,128)(2,1)} async-done(((bf16[512,512]{1,0:T(8,128)(2,1)}), bf16[512,4096]{1,0:T(8,128)(2,1)}) %all-gather.7.cloned.1.call-update) | async-done | bytes 4194320 | tf_op jit(solution)/shard_map/all_gather | solution.py:155
  271.9 3.7 convolution_convert_fusion.2
  275.6 2.9 fusion.5
  278.6 5.9 %convolution_convert_fusion = bf16[128,4096]{1,0:T(8,128)(2,1)} fusion(bf16[1,512,4096]{2,1,0:T(8,128)(2,1)} %param.37, bf16[128,4096]{1,0:T(8,128)(2,1)S(1)} %bitcast.73, bf16[1,4096,512]{2,1,0:T(8,128)(2,1)} %param.36, f32[128,512]{1,0:T(8,128)S(1)} %fusion.5), kind=kOutput, calls=%fused_computation | convolution fusion | flops 1074659328 | bytes 10747904 | tf_op jit(solution)/shard_map/dot_general | solution.py:130
  284.5 55.4 %all-reduce.3.cloned.1.call-done = (bf16[8,16,4096]{2,1,0:T(8,128)(2,1)}, bf16[32,4096]{1,0:T(8,128)(2,1)}) async-done(((bf16[8,16,4096]{2,1,0:T(8,128)(2,1)}, bf16[32,4096]{1,0:T(8,128)(2,1)}), (bf16[8,16,4096]{2,1,0:T(8,128)(2,1)}, bf16[32,4096]{1,0:T(8,128)(2,1)})) %all-reduce.3.cloned.1.call-update) | async-done | bytes 1310736 | tf_op jit(solution)/shard_map/psum | solution.py:131
  339.8 4.6 %all-to-all-start.2 = ((bf16[8,16,4096]{2,1,0:T(8,128)(2,1)}), bf16[8,16,4096]{2,1,0:T(8,128)(2,1)S(1)}, u32[]{:S(2)}, u32[]{:S(2)}) async-start(bf16[8,16,4096]{2,1,0:T(8,128)(2,1)} %get-tuple-element.3), calls=%async_computation.3 | async-start | bytes 2097152 | tf_op jit(solution)/shard_map/all_to_all | solution.py:132
  344.5 0.7 fusion.45
  345.4 0.2 fusion.27
  345.6 25.4 %all-to-all-done.2 = bf16[8,16,4096]{2,1,0:T(8,128)(2,1)S(1)} async-done(((bf16[8,16,4096]{2,1,0:T(8,128)(2,1)}), bf16[8,16,4096]{2,1,0:T(8,128)(2,1)S(1)}, u32[]{:S(2)}, u32[]{:S(2)}) %all-to-all-start.2) | async-done | bytes 1048608 | tf_op jit(solution)/shard_map/all_to_all | solution.py:132
  371.0 2.0 fusion.1
  (68 shorter events, 2.3 us)
Async XLA Ops:
  7.2 54.7 %copy-start = (bf16[16,64,64]{2,1,0:T(8,128)(2,1)S(1)}, bf16[16,64,64]{2,1,0:T(8,128)(2,1)}, u32[]{:S(2)}) copy-start(bf16[16,64,64]{2,1,0:T(8,128)(2,1)} %param.28) | copy-start | bytes 393220
  7.2 53.5 %reduce-scatter.3.cloned.1.call-start = ((), (), s32[]{:S(2)}) async-start(), calls=%async_computation.6 | async-start | bytes 1179648 | tf_op jit(solution)/shard_map/reduce_scatter | solution.py:54
  8.4 21.3 %copy-start.11 = (f32[1024]{0:T(1024)S(1)}, f32[1024]{0:T(1024)}, u32[]{:S(2)}) copy-start(f32[1024]{0:T(1024)} %param.30) | copy-start | bytes 12292
  9.5 52.1 %copy-start.3 = (bf16[32,3,1024]{2,0,1:T(8,128)(2,1)S(1)}, bf16[32,3,1024]{2,0,1:T(8,128)(2,1)}, u32[]{:S(2)}) copy-start(bf16[32,3,1024]{2,0,1:T(8,128)(2,1)} %param.23) | copy-start | bytes 589828
  9.5 52.1 %copy-start.8 = (f32[4,1024]{1,0:T(4,128)S(1)}, f32[4,1024]{1,0:T(4,128)}, u32[]{:S(2)}) copy-start(f32[4,1024]{1,0:T(4,128)} %param.27) | copy-start | bytes 49156
  25.5 36.8 %copy-start.14 = (bf16[16,64,64]{2,1,0:T(8,128)(2,1)S(1)}, bf16[16,64,64]{2,1,0:T(8,128)(2,1)}, u32[]{:S(2)}) copy-start(bf16[16,64,64]{2,1,0:T(8,128)(2,1)} %param.29) | copy-start | bytes 393220
  28.9 34.0 %copy-start.5 = (f32[32,1024]{1,0:T(8,128)S(1)}, f32[32,1024]{1,0:T(8,128)}, u32[]{:S(2)}) copy-start(f32[32,1024]{1,0:T(8,128)} %param.22) | copy-start | bytes 393220
  28.9 113.6 %all-gather.5.cloned.1.call-start = ((), (), s32[]{:S(2)}) async-start(), calls=%async_computation.7 | async-start | bytes 9437184 | tf_op jit(solution)/shard_map/all_gather | solution.py:84
  29.7 143.6 %all-gather.9.cloned.1.call-start = ((), (), s32[]{:S(2)}) async-start(), calls=%async_computation.10 | async-start | bytes 1310720 | tf_op jit(solution)/shard_map/all_gather | solution.py:13
  60.7 81.8 %copy-start.4 = (bf16[32,2048]{1,0:T(8,128)(2,1)S(1)}, bf16[32,2048]{1,0:T(8,128)(2,1)}, u32[]{:S(2)}) copy-start(bf16[32,2048]{1,0:T(8,128)(2,1)} %reduce-scatter.3.cloned.1.call-done) | copy-start | bytes 393220
  63.0 85.1 %copy-start.2 = (f32[32,1024]{1,0:T(8,128)}, f32[32,1024]{1,0:T(8,128)S(1)}, u32[]{:S(2)}) copy-start(f32[32,1024]{1,0:T(8,128)S(1)} %multiply_add_fusion) | copy-start | bytes 393220
  63.0 111.7 %copy-start.1 = (bf16[32,4096]{1,0:T(8,128)(2,1)S(1)}, bf16[32,4096]{1,0:T(8,128)(2,1)}, u32[]{:S(2)}) copy-start(bf16[32,4096]{1,0:T(8,128)(2,1)} %param.21) | copy-start | bytes 786436
  63.0 111.9 %copy-start.7 = (f32[4096]{0:T(1024)S(1)}, f32[4096]{0:T(1024)}, u32[]{:S(2)}) copy-start(f32[4096]{0:T(1024)} %param.32) | copy-start | bytes 49156
  63.0 126.2 %copy-start.12 = (bf16[512,512]{1,0:T(8,128)(2,1)S(1)}, bf16[512,512]{1,0:T(8,128)(2,1)}, u32[]{:S(2)}) copy-start(bf16[512,512]{1,0:T(8,128)(2,1)} %param.39) | copy-start | bytes 1572868
  63.0 126.2 %copy-start.13 = (bf16[512,512]{1,0:T(8,128)(2,1)S(1)}, bf16[512,512]{1,0:T(8,128)(2,1)}, u32[]{:S(2)}) copy-start(bf16[512,512]{1,0:T(8,128)(2,1)} %param.38) | copy-start | bytes 1572868
  148.1 43.0 %copy-start.9 = (s32[32,2]{0,1:T(2,128)S(1)}, s32[32,2]{0,1:T(2,128)}, u32[]{:S(2)}) copy-start(s32[32,2]{0,1:T(2,128)} %param.34) | copy-start | bytes 772
  148.2 73.2 %reduce-scatter.5.cloned.1.call-start = ((), (), s32[]{:S(2)}) async-start(), calls=%async_computation.8 | async-start | bytes 589824 | tf_op jit(solution)/shard_map/reduce_scatter | solution.py:142
  190.5 81.4 %all-gather.7.cloned.1.call-start = ((), (), s32[]{:S(2)}) async-start(), calls=%async_computation.9 | async-start | bytes 4718592 | tf_op jit(solution)/shard_map/all_gather | solution.py:155
  193.3 82.4 %all-to-all-start.1 = ((bf16[8,16,4096]{2,1,0:T(8,128)(2,1)}), bf16[8,16,4096]{2,1,0:T(8,128)(2,1)S(1)}, u32[]{:S(2)}, u32[]{:S(2)}) async-start(bf16[8,16,4096]{2,1,0:T(8,128)(2,1)} %bitcast.10), calls=%async_computation.2 | async-start | bytes 2097152 | tf_op jit(solution)/shard_map/all_to_all | solution.py:124
  196.8 143.0 %all-reduce.3.cloned.1.call-start = ((), (), s32[]{:S(2)}) async-start(), calls=%async_computation.11 | async-start | bytes 2621440 | tf_op jit(solution)/shard_map/psum | solution.py:131
  278.5 65.9 %copy-start.10 = (bf16[4096]{0:T(1024)(128)(2,1)S(1)}, bf16[4096]{0:T(1024)(128)(2,1)}, u32[]{:S(2)}) copy-start(bf16[4096]{0:T(1024)(128)(2,1)} %param.41) | copy-start | bytes 24580
  278.6 66.6 %copy-start.6 = (bf16[4096,8]{0,1:T(8,128)(2,1)S(1)}, bf16[4096,8]{0,1:T(8,128)(2,1)}, u32[]{:S(2)}) copy-start(bf16[4096,8]{0,1:T(8,128)(2,1)} %param.33) | copy-start | bytes 196612
  339.8 31.2 %all-to-all-start.2 = ((bf16[8,16,4096]{2,1,0:T(8,128)(2,1)}), bf16[8,16,4096]{2,1,0:T(8,128)(2,1)S(1)}, u32[]{:S(2)}, u32[]{:S(2)}) async-start(bf16[8,16,4096]{2,1,0:T(8,128)(2,1)} %get-tuple-element.3), calls=%async_computation.3 | async-start | bytes 2097152 | tf_op jit(solution)/shard_map/all_to_all | solution.py:132
Sparse Core Ops, SparseCore 0:
  29.0 31.6 reduce-scatter.2
  62.3 80.1 all-gather.4
  148.3 24.9 all-gather.8
  190.6 30.6 reduce-scatter.4
  222.8 49.0 all-gather.6
  284.6 55.1 all-reduce.2
